TPU v7x, 32 devices: a whole 2x2x4 slice. The times are simulated.
32 devices in a mesh: grp: 2 (over y), sp: 4 (over z), tp: 4 (over x, core).
Axes of the slice: x: 2, y: 2, z: 4, core: 2. Of those that a mesh axis runs over, the one named last changes fastest.
Arguments:
- tokens: bfloat16 [1024, 2048], P(('grp', 'sp')), parts along dimension 0, may hold values from -6 to 6
- norm_gain: float32 [2048], replicated, may hold values from 0.1 to 1.9
- w_query: bfloat16 [2048, 512], P('sp', 'tp'), may hold values from -0.125 to 0.125
- w_key: bfloat16 [2048, 512], P('sp', 'tp'), may hold values from -0.125 to 0.125
- w_value: bfloat16 [2048, 512], P('sp', 'tp'), may hold values from -0.125 to 0.125
- w_glu_value: bfloat16 [2048, 1024], P('sp', 'tp'), may hold values from -0.125 to 0.125
- w_glu_gate: bfloat16 [2048, 1024], P('sp', 'tp'), may hold values from -0.125 to 0.125
- key_offset: bfloat16 [1024, 8], P(('grp', 'sp'), 'tp'), parts along dimension 0, may hold values from -13 to 0
- head_gain: float32 [8, 64], P('tp'), may hold values from 0.1 to 1.9
- conv_taps: float32 [31, 1024], P(None, 'tp'), may hold values from -2.873685 to 2.873685
- channel_gain: float32 [1024], P('tp'), may hold values from 0.1 to 1.9
- channel_bias: float32 [1024], P('tp'), may hold values from -3 to 3
- w_out_attn: bfloat16 [512, 2048], P('tp'), may hold values from -0.15625 to 0.15625
- w_out_conv: bfloat16 [1024, 2048], P('tp'), may hold values from -0.15625 to 0.15625
- out_gain: float32 [2048], replicated, may hold values from 0.1 to 1.9
Outputs:
- mixed: bfloat16 [1024, 2048], P(('grp', 'sp')), parts along dimension 0
- log_mass: float32 [8, 1024], P('tp', ('grp', 'sp')), parts along dimension 1
There are 2 independent parts, one for each index of `grp`. A program takes and returns all parts, laid end to end along the dimension named above; an argument that names none is the same for every part. Nothing has to cross between parts.
All inputs are finite; a program needn't handle non-finite values.
Results may differ from a plain program's by a relative error of at most 0.011.
Values may be sent and summed in bfloat16 or wider, within the bound.
A program may use at most 64 MiB of HBM per device.

v0:
```python
import jax
import jax.numpy as jnp
from jax import lax
from jax.sharding import PartitionSpec as P

HD = 64
CW = 1024


norm_eps = 1e-06


def from_behind(value, axis, steps):
    count = lax.axis_size(axis)
    initial, last = (max(0, -steps), min(count, count - steps))
    return lax.ppermute(value, axis, [(source, source + steps) for source in range(initial, last)])


def row_norm(values_in, gain_vec):
    squares = jnp.mean(values_in * values_in, axis=-1, keepdims=True)
    return values_in * lax.rsqrt(squares + norm_eps) * gain_vec


def local(
    tokens,
    norm_gain,
    w_query,
    w_key,
    w_value,
    w_glu_value,
    w_glu_gate,
    key_offset,
    head_gain,
    conv_taps,
    channel_gain,
    channel_bias,
    w_out_attn,
    w_out_conv,
    out_gain,
):
    row_count = tokens.shape[0]
    normed = row_norm(tokens.astype(jnp.float32), norm_gain).astype(jnp.bfloat16)
    weights_in = (w_query, w_key, w_value, w_glu_value, w_glu_gate)
    pieces = (
        lax.all_gather(weights_in[0], "sp", axis=0, tiled=True),
        lax.all_gather(weights_in[1], "sp", axis=0, tiled=True),
        lax.all_gather(weights_in[2], "sp", axis=0, tiled=True),
        lax.all_gather(weights_in[3], "sp", axis=0, tiled=True),
        lax.all_gather(weights_in[4], "sp", axis=0, tiled=True),
    )
    projected = tuple(
        (jnp.dot(normed, shard_piece, preferred_element_type=jnp.float32) for shard_piece in pieces)
    )
    query, key_rows, value_rows, glu_value, glu_gate = [
        summed.astype(jnp.bfloat16) for summed in projected
    ]
    kv_local = key_rows.shape[1] // HD
    group_size = query.shape[1] // key_rows.shape[1]
    heads_local = kv_local * group_size
    all_keys, all_values, all_offsets = (
        lax.all_gather(key_rows, "sp", axis=0, tiled=True),
        lax.all_gather(value_rows, "sp", axis=0, tiled=True),
        lax.all_gather(key_offset, "sp", axis=0, tiled=True),
    )
    sequence_length_total = all_keys.shape[0]
    shard_count = lax.axis_size("sp")
    per_block = 1
    while (
        per_block * 2 <= shard_count
        and shard_count % (per_block * 2) == 0
        and (per_block * 2 * row_count <= 1024)
    ):
        per_block = per_block * 2
    span_len = per_block * row_count
    query_heads = query.reshape(row_count, kv_local, group_size, HD)
    key_heads = all_keys.reshape(sequence_length_total, kv_local, HD)
    value_heads = all_values.reshape(sequence_length_total, kv_local, HD)
    my_index = lax.axis_index("sp")
    query_pos = my_index * row_count + jnp.arange(row_count, dtype=jnp.int32)
    last_block = my_index // per_block
    zeros_mix = jnp.zeros((kv_local, group_size, row_count, HD), jnp.float32)
    zeros_row = jnp.zeros((kv_local, group_size, row_count), jnp.float32)

    def sweep(turn_index, carry):
        head_mix, mass_sum, carried = carry
        first_key = (last_block - turn_index) * span_len
        key_block = lax.dynamic_slice_in_dim(key_heads, first_key, span_len, 0)
        value_block = lax.dynamic_slice_in_dim(value_heads, first_key, span_len, 0)
        offset_block = lax.dynamic_slice_in_dim(all_offsets, first_key, span_len, 0).astype(
            jnp.float32
        )
        offset_block = offset_block.T.reshape(kv_local, group_size, 1, span_len)
        scores = (
            jnp.einsum("qhgd,khd->hgqk", query_heads, key_block, preferred_element_type=jnp.float32)
            * HD ** (-0.5)
            + offset_block
        )
        key_pos = first_key + jnp.arange(span_len, dtype=jnp.int32)
        allowed = key_pos[None, :] <= query_pos[:, None]
        log_not = jnp.where(allowed, jax.nn.log_sigmoid(-scores), 0.0)
        later = lax.cumsum(log_not, axis=3, reverse=True) - log_not + carried[..., None]
        weights = jnp.where(allowed, jnp.exp(jax.nn.log_sigmoid(scores) + later), 0.0)
        head_mix = head_mix + jnp.einsum(
            "hgqk,khd->hgqd",
            weights.astype(jnp.bfloat16),
            value_block,
            preferred_element_type=jnp.float32,
        )
        return (head_mix, mass_sum + jnp.sum(weights, axis=3), carried + jnp.sum(log_not, axis=3))

    head_mix, mass_sum, leftover = lax.fori_loop(
        0, last_block + 1, sweep, (zeros_mix, zeros_row, zeros_row)
    )
    log_mass = jnp.log(mass_sum).reshape(heads_local, row_count)
    head_rows = head_mix.transpose(2, 0, 1, 3).reshape(row_count, heads_local, HD)
    attended = (
        row_norm(head_rows, head_gain).astype(jnp.bfloat16).reshape(row_count, heads_local * HD)
    )
    gated = (glu_value.astype(jnp.float32) * jax.nn.sigmoid(glu_gate.astype(jnp.float32))).astype(
        jnp.bfloat16
    )
    reach_len = conv_taps.shape[0] - 1
    before = from_behind(gated[row_count - reach_len :], "sp", 1)
    padded = jnp.concatenate([before, gated], axis=0).astype(jnp.float32)
    conv_out = jnp.zeros(gated.shape, jnp.float32)
    for tap_index in range(conv_taps.shape[0]):
        conv_out = conv_out + conv_taps[tap_index] * padded[tap_index : tap_index + row_count]
    total_sum, total_squares = lax.psum(
        (jnp.sum(conv_out, axis=1), jnp.sum(conv_out * conv_out, axis=1)), "tp"
    )
    chan_mean = (total_sum / CW)[:, None]
    spread = (total_squares / CW)[:, None] - chan_mean * chan_mean
    centered = conv_out - chan_mean
    channel_out = jax.nn.silu(
        centered * lax.rsqrt(spread + norm_eps) * channel_gain + channel_bias
    ).astype(jnp.bfloat16)
    share = lax.psum_scatter(
        jnp.dot(attended, w_out_attn, preferred_element_type=jnp.float32)
        + jnp.dot(channel_out, w_out_conv, preferred_element_type=jnp.float32),
        "tp",
        scatter_dimension=0,
        tiled=True,
    )
    mixed = lax.all_gather(row_norm(share, out_gain).astype(jnp.bfloat16), "tp", axis=0, tiled=True)
    return (mixed, log_mass)


def solution(mesh):
    in_specs = (
        P(("grp", "sp"), None),
        P(),
        P("sp", "tp"),
        P("sp", "tp"),
        P("sp", "tp"),
        P("sp", "tp"),
        P("sp", "tp"),
        P(("grp", "sp"), "tp"),
        P("tp", None),
        P(None, "tp"),
        P("tp"),
        P("tp"),
        P("tp", None),
        P("tp", None),
        P(),
    )
    out_specs = (P(("grp", "sp"), None), P("tp", ("grp", "sp")))
    return jax.shard_map(local, mesh=mesh, in_specs=in_specs, out_specs=out_specs, check_vma=False)
```

profile of v0, /device:TPU:0, one launch (start us, length us, event | category | flops | bytes accessed | tf_op | source)
XLA Modules:
  0.0 168.1 jit_solution(18097645065637768242)
XLA Ops:
  8.0 0.7 all-gather.5.cloned.1.call-update
  9.0 0.7 copy-done.4
  9.7 21.4 %all_gather.28 = bf16[2048,128]{1,0:T(8,128)(2,1)S(1)} all-gather(bf16[512,128]{1,0:T(8,128)(2,1)S(1)} %copy-done.4), channel_id=1, replica_groups=mesh['grp'=2,'sp'=4,'tp'=4] {'sp'}, dimensions={0}, use_global_device_ids=true | all-gather | bytes 655360 | tf_op jit(solution)/shard_map/all_gather | solution.py:46
  31.4 14.8 %all_gather.29 = bf16[512,128]{1,0:T(8,128)(2,1)S(1)} all-gather(bf16[128,128]{1,0:T(8,128)(2,1)S(1)} %convolution_convert_fusion.3), channel_id=1, replica_groups=mesh['grp'=2,'sp'=4,'tp'=4] {'sp'}, dimensions={0}, use_global_device_ids=true | all-gather | bytes 163840 | tf_op jit(solution)/shard_map/all_gather | solution.py:61
  46.4 0.8 copy-done.5
  47.2 18.3 %all_gather.31 = bf16[2048,128]{1,0:T(8,128)(2,1)S(1)} all-gather(bf16[512,128]{1,0:T(8,128)(2,1)S(1)} %copy-done.5), channel_id=1, replica_groups=mesh['grp'=2,'sp'=4,'tp'=4] {'sp'}, dimensions={0}, use_global_device_ids=true | all-gather | bytes 655360 | tf_op jit(solution)/shard_map/all_gather | solution.py:47
  65.8 15.0 %all_gather.32 = bf16[512,128]{1,0:T(8,128)(2,1)S(1)} all-gather(bf16[128,128]{1,0:T(8,128)(2,1)S(1)} %convolution_convert_fusion.2), channel_id=1, replica_groups=mesh['grp'=2,'sp'=4,'tp'=4] {'sp'}, dimensions={0}, use_global_device_ids=true | all-gather | bytes 163840 | tf_op jit(solution)/shard_map/all_gather | solution.py:62
  81.0 0.8 copy-done.6
  81.8 14.7 %all_gather.27 = bf16[2048,128]{1,0:T(8,128)(2,1)S(1)} all-gather(bf16[512,128]{1,0:T(8,128)(2,1)S(1)} %copy-done.6), channel_id=1, replica_groups=mesh['grp'=2,'sp'=4,'tp'=4] {'sp'}, dimensions={0}, use_global_device_ids=true | all-gather | bytes 655360 | tf_op jit(solution)/shard_map/all_gather | solution.py:45
  97.5 9.8 %all_gather.30 = bf16[512,2]{0,1:T(2,128)(2,1)S(1)} all-gather(bf16[128,2]{0,1:T(2,128)(2,1)S(1)} %copy-done.11), channel_id=1, replica_groups=mesh['grp'=2,'sp'=4,'tp'=4] {'sp'}, dimensions={0}, use_global_device_ids=true | all-gather | bytes 2560 | tf_op jit(solution)/shard_map/all_gather | solution.py:63
  107.3 4.3 %while.15 = (s32[]{:T(128)}, f32[2,1,128,64]{2,3,0,1:T(8,128)S(1)}, f32[2,1,128]{2,1,0:T(1,128)S(1)}, f32[2,1,128]{2,0,1:T(2,128)S(1)}, s32[]{:T(128)}, /*index=...) while((s32[]{:T(128)}, f32[2,1,128,64]{2,3,0,1:T(8,128)S(1)}, ...), condition=%wide.region_6.7_spmd.clone, body=%wide.region_1.6_spmd.clone.sunk | while | flops 54744452 | bytes 5395625 | solution.py:111
  108.0 2.4 %fusion.105 = f32[2,1,128,4,128]{2,3,4,1,0:T(4,128)S(1)} fusion(f32[2,1,128,4,128]{2,4,3,0,1:T(8,128)S(1)} %bitcast.128), kind=kOutput, calls=%fused_computation.18.clone.1 | output fusion | flops 16646144 | bytes 1048576 | tf_op jit(solution)/shard_map/reduce-window
  110.5 0.8 fusion.106
  111.6 0.7 copy-done.7
  112.3 1.6 fusion.27
  114.0 1.6 fusion.26
  115.6 1.7 %collective-permute-start = (bf16[30,256]{1,0:T(8,128)(2,1)S(1)}, bf16[30,256]{1,0:T(8,128)(2,1)S(1)}, u32[]{:S(2)}, u32[]{:S(2)}) collective-permute-start(bf16[30,256]{1,0:T(8,128)(2,1)S(1)} %slice.262), channel_id=1, source_target_pairs={{0,4},{4,8},{8,12},{1,5},{5,9},{9,13},{2,6},{6,10},{10,14},{3,7},{... | collective-permute-start | bytes 46088 | tf_op jit(solution)/shard_map/ppermute | solution.py:16
  117.5 1.2 collective-permute-done
  119.4 5.7 %all-reduce = (f32[128]{0:T(128)S(1)}, f32[128]{0:T(128)S(1)}) all-reduce(f32[128]{0:T(128)S(1)} %get-tuple-element.112, f32[128]{0:T(128)S(1)} %get-tuple-element.111), channel_id=1, replica_groups=mesh['grp'=2,'sp'=4,'tp'=4] {'tp'}, use_global_device_ids=true, to_apply=%region_11.12 | all-reduce | flops 256 | bytes 2048 | tf_op jit(solution)/shard_map/psum | solution.py:128
  126.8 1.3 convolution_add_fusion
  128.7 24.2 %reduce-scatter.2.cloned.1.call-done = f32[32,2048]{1,0:T(8,128)} async-done(((f32[128,2048]{1,0:T(8,128)}), f32[32,2048]{1,0:T(8,128)}) %reduce-scatter.2.cloned.1.call-update) | async-done | bytes 262160 | tf_op jit(solution)/shard_map/reduce_scatter | solution.py:137
  152.9 1.1 multiply_reduce_fusion
  154.1 6.6 %all_gather.35 = bf16[128,2048]{1,0:T(8,128)(2,1)S(1)} all-gather(bf16[32,2048]{1,0:T(8,128)(2,1)S(1)} %multiply_convert_fusion), channel_id=1, replica_groups=mesh['grp'=2,'sp'=4,'tp'=4] {'tp'}, dimensions={0}, use_global_device_ids=true | all-gather | bytes 655360 | tf_op jit(solution)/shard_map/all_gather | solution.py:144
  160.7 0.8 copy.53
  (67 shorter events, 7.3 us)
Async XLA Ops:
  7.2 117.9 %copy-start = (bf16[256,2048]{1,0:T(8,128)(2,1)S(1)}, bf16[256,2048]{1,0:T(8,128)(2,1)}, u32[]{:S(2)}) copy-start(bf16[256,2048]{1,0:T(8,128)(2,1)} %param.30) | copy-start | bytes 3145732
  7.2 1.6 copy-start.2
  7.2 105.2 %all-gather.3.cloned.1.call-start = ((), (), s32[]{:S(2)}) async-start(), calls=%async_computation.1 | async-start | bytes 1310720 | tf_op jit(solution)/shard_map/all_gather | solution.py:48
  7.9 106.0 %all-gather.5.cloned.1.call-start = ((), (), s32[]{:S(2)}) async-start(), calls=%async_computation.2 | async-start | bytes 1310720 | tf_op jit(solution)/shard_map/all_gather | solution.py:49
  8.7 144.2 %reduce-scatter.2.cloned.1.call-start = ((), (), s32[]{:S(2)}) async-start(), calls=%async_computation.3 | async-start | bytes 1310720 | tf_op jit(solution)/shard_map/reduce_scatter | solution.py:137
  8.7 0.9 copy-start.4
  9.7 21.4 %copy-start.12 = (f32[2048]{0:T(1024)S(1)}, f32[2048]{0:T(1024)}, u32[]{:S(2)}) copy-start(f32[2048]{0:T(1024)} %param.18) | copy-start | bytes 24580
  46.2 0.9 copy-start.5
  80.8 0.9 copy-start.6
  96.8 0.7 copy-start.11
  111.5 0.8 copy-start.7
  115.6 1.8 %copy-start.13 = (f32[2,64]{1,0:T(2,128)S(1)}, f32[2,64]{1,0:T(2,128)}, u32[]{:S(2)}) copy-start(f32[2,64]{1,0:T(2,128)} %param.25) | copy-start | bytes 1540
  115.6 3.2 %collective-permute-start = (bf16[30,256]{1,0:T(8,128)(2,1)S(1)}, bf16[30,256]{1,0:T(8,128)(2,1)S(1)}, u32[]{:S(2)}, u32[]{:S(2)}) collective-permute-start(bf16[30,256]{1,0:T(8,128)(2,1)S(1)} %slice.262), channel_id=1, source_target_pairs={{0,4},{4,8},{8,12},{1,5},{5,9},{9,13},{2,6},{6,10},{10,14},{3,7},{... | collective-permute-start | bytes 46088 | tf_op jit(solution)/shard_map/ppermute | solution.py:16
  118.8 6.3 %copy-start.10 = (f32[256]{0:T(256)S(1)}, f32[256]{0:T(256)}, u32[]{:S(2)}) copy-start(f32[256]{0:T(256)} %param.27) | copy-start | bytes 3076
  125.0 0.7 copy-start.9
  125.7 1.0 copy-start.3
  128.1 26.0 %copy-start.8 = (f32[2048]{0:T(1024)S(1)}, f32[2048]{0:T(1024)}, u32[]{:S(2)}) copy-start(f32[2048]{0:T(1024)} %param.31) | copy-start | bytes 24580
  152.9 1.2 copy-start.1
Sparse Core Ops, SparseCore 0:
  9.6 35.8 all-gather.2
  47.1 34.8 all-gather.4
  128.2 24.6 reduce-scatter.1
where the time goes:
time: 169 us; the launch traced here: 168 us
  blocking collectives  106 us (63%)
  waiting for transfers between devices  26.9 us (16%)
  between operations  14 us (8%)
  local copies, waits for them, and re-layouts  6.76 us (4%)
  matrix products  6.76 us (4%)
  other arithmetic  5.54 us (3%)
  starting transfers between devices  1.83 us (1%)
    reduce_scatter x1, waiting for transfers between devices, local(): lax.psum_scatter(jnp.dot(attended, w_out_attn, preferred_element_type=jnp...  24.2 us
    all_gather x1, blocking collectives, local(): lax.all_gather(weights_in[1], 'sp', axis=0, tiled=True)  21.4 us
    all_gather x1, blocking collectives, local(): lax.all_gather(weights_in[2], 'sp', axis=0, tiled=True)  18.3 us
    all_gather x1, blocking collectives, local(): lax.all_gather(value_rows, 'sp', axis=0, tiled=True)  15 us
    all_gather x1, blocking collectives, local(): lax.all_gather(key_rows, 'sp', axis=0, tiled=True)  14.8 us
    all_gather x1, blocking collectives, local(): lax.all_gather(weights_in[0], 'sp', axis=0, tiled=True)  14.7 us
    all_gather x1, blocking collectives, local(): lax.all_gather(key_offset, 'sp', axis=0, tiled=True)  9.75 us
    all_gather x1, blocking collectives, local(): lax.all_gather(row_norm(share, out_gain).astype(jnp.bfloat16), 'tp', axis...  6.6 us
  transfers between devices with their start and end apart: 4, of which 2 were waited for; matrix products, arithmetic and copies ran while one was open for 5% of the time, Pallas kernels for 0%

commit v1 on v0

--- a/solution.py
+++ b/solution.py
@@ -1,6 +1,10 @@
+import functools
+
 import jax
 import jax.numpy as jnp
 from jax import lax
+from jax.experimental import pallas as pl
+from jax.experimental.pallas import tpu as pltpu
 from jax.sharding import PartitionSpec as P
 
 HD = 64
@@ -145,6 +149,691 @@
     return (mixed, log_mass)
 
 
+F32 = jnp.float32
+BF16 = jnp.bfloat16
+MESH = pl.DeviceIdType.MESH
+
+
+def split_kernel(
+    SP,
+    tokens,
+    norm_gain,
+    w_query,
+    w_key,
+    w_value,
+    w_gv,
+    w_gg,
+    key_offset,
+    head_gain,
+    conv_taps,
+    channel_gain,
+    channel_bias,
+    w_oa,
+    w_oc,
+    out_gain,
+    out,
+    log_out,
+    X,
+    WA,
+    stg,
+    prm,
+    offs,
+    offr,
+    proj,
+    gp,
+    snd,
+    lms,
+    sts,
+    ar,
+    cr,
+    lmr,
+    sr,
+    woa,
+    woc,
+    mp,
+    ma,
+    bx,
+    bxr,
+    s_wo,
+    s_ws,
+    s_wr,
+    s_wys,
+    s_wyr,
+    s_xl,
+    s_xrt,
+    s_xr,
+    s_xxs,
+    s_xxr,
+    s_xds,
+    s_xdr,
+    s_ps,
+    s_pr,
+    s_os,
+    s_or,
+    s_ds,
+    s_dr,
+    s_ls,
+    s_lr,
+    s_ss,
+    s_sr,
+    s_ms,
+    s_mr,
+    s_bs,
+    s_br,
+    s_es,
+    s_er,
+):
+    g = lax.axis_index("grp")
+    z = lax.axis_index("sp")
+    tp = lax.axis_index("tp")
+    x = tp // 2
+    c = tp % 2
+    partner = 2 * x + (1 - c)
+    across = 2 * (1 - x) + c
+    diag = 2 * (1 - x) + (1 - c)
+    mine = z // 2
+    par = z % 2
+    R = tokens.shape[0]
+    D = tokens.shape[1]
+    KS = w_query.shape[0]
+    KH = KS // 2
+    Q = R // 4
+    taps_n = conv_taps.shape[0]
+
+    def rc(src, dst, ss, rs, dev):
+        return pltpu.make_async_remote_copy(
+            src_ref=src, dst_ref=dst, send_sem=ss, recv_sem=rs, device_id=dev, device_id_type=MESH
+        )
+
+    wo_a = pltpu.make_async_copy(w_oa, woa, s_wo.at[0])
+    wo_c = pltpu.make_async_copy(w_oc, woc, s_wo.at[1])
+    wo_a.start()
+    wo_c.start()
+
+    barrier = pltpu.get_barrier_semaphore()
+    for dz in range(SP):
+        for dt in range(4):
+            if dz == 0 and dt == 0:
+                continue
+            pl.semaphore_signal(
+                barrier, inc=1, device_id=(g, (z + dz) % SP, (tp + dt) % 4), device_id_type=MESH
+            )
+    pl.semaphore_signal(barrier, inc=1, device_id=(1 - g, z, tp), device_id_type=MESH)
+
+    t32 = tokens[...].astype(F32)
+    sq = jnp.mean(t32 * t32, axis=-1, keepdims=True)
+    X[pl.ds(pl.multiple_of(z * R, R), R), :] = (
+        t32 * lax.rsqrt(sq + norm_eps) * norm_gain[...]
+    ).astype(BF16)
+    pl.semaphore_wait(barrier, SP * 4)
+
+    def xs(block, quarter):
+        return X.at[pl.ds(pl.multiple_of(block * R + quarter * Q, Q), Q), :]
+
+    def x_right(b):
+        return rc(xs(b, tp), xs(b, tp), s_xrt.at[b], s_xr.at[b], (g, jnp.minimum(z + 1, SP - 1), tp))
+
+    def x_left(b):
+        return rc(xs(b, tp), xs(b, tp), s_xl.at[b], s_xr.at[b], (g, jnp.maximum(z - 1, 0), tp))
+
+    def x_cross(b):
+        return rc(xs(b, tp), xs(b, tp), s_xxs.at[b], s_xxr.at[b], (g, z, across))
+
+    def x_cross_in(b):
+        return rc(xs(b, across), xs(b, across), s_xxs.at[b], s_xxr.at[b], (g, z, across))
+
+    def x_d2d(b, k, quarter):
+        return rc(xs(b, quarter), xs(b, quarter), s_xds.at[b, k], s_xdr.at[b, k], (g, z, partner))
+
+    @pl.when(z < SP - 1)
+    def _():
+        x_right(z).start()
+
+    @pl.when(z > 0)
+    def _():
+        x_left(z).start()
+
+    for h in range(2):
+        stg[h, 0, :, 0:128] = jnp.concatenate(
+            [w_query[:, 64 * h : 64 * h + 64], w_key[:, 64 * h : 64 * h + 64]], axis=1
+        )
+        stg[h, 0, :, 128:256] = w_value[...]
+        stg[h, 1, :, 0:128] = w_gv[:, 128 * h : 128 * h + 128]
+        stg[h, 1, :, 128:256] = w_gg[:, 128 * h : 128 * h + 128]
+
+    def w_half(b, part):
+        return WA.at[pl.ds(pl.multiple_of(b * KS + part * KH, KH), KH), :]
+
+    def w_full(b):
+        return WA.at[pl.ds(pl.multiple_of(b * KS, KS), KS), :]
+
+    def w_far(h, r):
+        return rc(
+            stg.at[h, r, pl.ds(pl.multiple_of(g * KH, KH), KH), :],
+            w_half(z, g),
+            s_ws.at[h, r],
+            s_wr.at[z],
+            (g, 2 * c + h, 2 * x + r),
+        )
+
+    def w_near(h, r):
+        return rc(stg.at[h, r], w_full(z), s_ws.at[h, r], s_wr.at[z], (g, z, partner))
+
+    def w_own(h, r):
+        return pltpu.make_async_copy(stg.at[h, r], w_full(z), s_wr.at[z])
+
+    for h in range(2):
+        for r in range(2):
+            zt = 2 * c + h
+
+            @pl.when(zt != z)
+            def _():
+                w_far(h, r).start()
+
+            @pl.when((zt == z) & (c != r))
+            def _():
+                w_near(h, r).start()
+
+            @pl.when((zt == z) & (c == r))
+            def _():
+                w_own(h, r).start()
+
+    eye = lax.broadcasted_iota(jnp.int32, (R, R), 0) == lax.broadcasted_iota(jnp.int32, (R, R), 1)
+
+    def to_row(col):
+        return jnp.broadcast_to(
+            jnp.sum(jnp.where(eye, jnp.broadcast_to(col, (R, R)), 0.0), axis=0, keepdims=True), (8, R)
+        )
+
+    def to_col(row):
+        return jnp.sum(jnp.where(eye, jnp.broadcast_to(row, (R, R)), 0.0), axis=1, keepdims=True)
+
+    def off_far(h):
+        return rc(offs.at[h], offr.at[z], s_os.at[h], s_or.at[z], (g, 2 * c + h, 2 * x))
+
+    def off_own(h):
+        return pltpu.make_async_copy(offs.at[h], offr.at[z], s_or.at[z])
+
+    ko = key_offset[...].astype(F32)
+    for h in range(2):
+        offs[h] = to_row(ko[:, h : h + 1])
+        own = (2 * c + h == z) & (c == 0)
+
+        @pl.when(own)
+        def _():
+            off_own(h).start()
+
+        @pl.when(jnp.logical_not(own))
+        def _():
+            off_far(h).start()
+
+    p_send = rc(prm, prm, s_ps.at[0], s_pr.at[0], (g, z, partner))
+
+    @pl.when(c == mine)
+    def _():
+        tt = jnp.where(par == 0, conv_taps[:, 0:128], conv_taps[:, 128:256])
+        prm[0:taps_n, :] = tt
+        prm[32:33, :] = jnp.concatenate([head_gain[0:1, :], head_gain[1:2, :]], axis=1)
+        p_send.start()
+
+    for d in range(1, SP):
+
+        @pl.when(z - d >= 0)
+        def _():
+            b = z - d
+            x_left(b).wait_recv()
+
+            @pl.when(z < SP - 1)
+            def _():
+                x_right(b).start()
+
+            x_cross(b).start()
+            x_d2d(b, 0, tp).start()
+
+        @pl.when(z + d < SP)
+        def _():
+            b = z + d
+            x_left(b).wait_recv()
+
+            @pl.when(z > 0)
+            def _():
+                x_left(b).start()
+
+            x_cross(b).start()
+            x_d2d(b, 0, tp).start()
+
+        for sgn in (-1, 1):
+
+            @pl.when((z + sgn * d >= 0) & (z + sgn * d < SP))
+            def _():
+                b = z + sgn * d
+                x_cross_in(b).wait_recv()
+                x_d2d(b, 1, across).start()
+
+        for sgn in (-1, 1):
+
+            @pl.when((z + sgn * d >= 0) & (z + sgn * d < SP))
+            def _():
+                b = z + sgn * d
+                w = rc(w_half(b, g), w_half(b, g), s_wys.at[b], s_wr.at[b], (1 - g, z, tp))
+                w.wait_recv()
+                rc(w_half(b, g), w_half(b, g), s_wys.at[b], s_wyr.at[b], (1 - g, z, tp)).start()
+
+    @pl.when(c == mine)
+    def _():
+        pltpu.make_async_copy(w_full(z), w_full(z), s_wr.at[z]).wait()
+
+    @pl.when(c != mine)
+    def _():
+        rc(w_full(z), w_full(z), s_ws.at[0, 0], s_wr.at[z], (g, z, partner)).wait_recv()
+        p_send.wait_recv()
+
+    for d in range(1, SP):
+        for sgn in (-1, 1):
+
+            @pl.when((z + sgn * d >= 0) & (z + sgn * d < SP))
+            def _():
+                b = z + sgn * d
+                x_d2d(b, 0, partner).wait_recv()
+                x_d2d(b, 1, diag).wait_recv()
+                rc(
+                    w_half(b, 1 - g), w_half(b, 1 - g), s_wys.at[b], s_wyr.at[b], (1 - g, z, tp)
+                ).wait_recv()
+
+    for b in range(SP):
+        proj[b * R : b * R + R, :] = jnp.dot(
+            X[b * R : b * R + R, :], WA[...], preferred_element_type=F32
+        ).astype(BF16)
+
+    def d_far(t, core):
+        buf = ar if core == 0 else cr
+        return rc(snd.at[t], buf.at[par], s_ds.at[t], s_dr.at[core, par], (g, t, 2 * x + mine))
+
+    def d_own(t, core):
+        buf = ar if core == 0 else cr
+        return pltpu.make_async_copy(snd.at[t], buf.at[par], s_dr.at[core, par])
+
+    def l_far(t):
+        return rc(lms.at[t], lmr.at[par], s_ls.at[t], s_lr.at[par], (g, t, 2 * x + mine))
+
+    def l_own(t):
+        return pltpu.make_async_copy(lms.at[t], lmr.at[par], s_lr.at[par])
+
+    def s_far(t, q):
+        return rc(sts.at[t], sr.at[4 * x + z], s_ss.at[t, q], s_sr.at[4 * x + z], (g, t, q))
+
+    def s_own(t):
+        return pltpu.make_async_copy(sts.at[t], sr.at[4 * x + z], s_sr.at[4 * x + z])
+
+    @pl.when(c == 0)
+    def _():
+        for s in range(SP):
+            own = (s == z) & (mine == 0)
+
+            @pl.when(own)
+            def _():
+                pltpu.make_async_copy(offr.at[s], offr.at[s], s_or.at[s]).wait()
+
+            @pl.when(jnp.logical_not(own))
+            def _():
+                rc(offr.at[s], offr.at[s], s_os.at[0], s_or.at[s], (g, z, partner)).wait_recv()
+
+        row_i = lax.broadcasted_iota(jnp.int32, (R, R), 0)
+        col_i = lax.broadcasted_iota(jnp.int32, (R, R), 1)
+        upper = jnp.where(row_i >= col_i, 1.0, 0.0).astype(BF16)
+        allowed = col_i <= row_i
+        lane_ok = (lax.broadcasted_iota(jnp.int32, (R, 128), 1) // 64) == par
+        for b in range(SP - 1, -1, -1):
+            q = proj[b * R : b * R + R, 0:64]
+            acc = jnp.zeros((R, 128), F32)
+            mass = jnp.zeros((R, 1), F32)
+            carried = jnp.zeros((R, 1), F32)
+            for kb in range(b, -1, -1):
+                k = proj[kb * R : kb * R + R, 64:128]
+                v = proj[kb * R : kb * R + R, 128:256]
+                v = jnp.where(lane_ok, v.astype(F32), 0.0).astype(BF16)
+                s = (
+                    lax.dot_general(q, k, (((1,), (1,)), ((), ())), preferred_element_type=F32)
+                    * HD ** (-0.5)
+                    + offr[kb, 0:1, :]
+                )
+                ln = -(jnp.maximum(s, 0.0) + jnp.log1p(jnp.exp(-jnp.abs(s))))
+                if kb == b:
+                    ln = jnp.where(allowed, ln, 0.0)
+                hi = ln.astype(BF16)
+                lo = (ln - hi.astype(F32)).astype(BF16)
+                incl = (
+                    jnp.dot(hi, upper, preferred_element_type=F32)
+                    + jnp.dot(lo, upper, preferred_element_type=F32)
+                    + carried
+                )
+                w = jnp.exp(s + incl)
+                if kb == b:
+                    w = jnp.where(allowed, w, 0.0)
+                carried = incl[:, 0:1]
+                mass = mass + jnp.sum(w, axis=1, keepdims=True)
+                acc = acc + jnp.dot(w.astype(BF16), v, preferred_element_type=F32)
+            ms = jnp.sum(acc * acc, axis=1, keepdims=True) / 64
+            snd[b] = (acc * lax.rsqrt(ms + norm_eps) * prm[32:33, :]).astype(BF16)
+            lms[b] = jnp.log(to_row(mass))
+            own = (b == z) & (mine == 0)
+
+            @pl.when(own)
+            def _():
+                d_own(b, 0).start()
+                l_own(b).start()
+
+            @pl.when(jnp.logical_not(own))
+            def _():
+                d_far(b, 0).start()
+                l_far(b).start()
+
+    @pl.when(c == 1)
+    def _():
+        gp[0:32, :] = jnp.zeros((32, 128), F32)
+        gv = proj[:, 0:128].astype(F32)
+        gg = proj[:, 128:256].astype(F32)
+        gp[32 : 32 + SP * R, :] = (gv * jax.nn.sigmoid(gg)).astype(BF16).astype(F32)
+        for b in range(SP):
+            conv = jnp.zeros((R, 128), F32)
+            for j in range(taps_n):
+                first = b * R + 32 - (taps_n - 1) + j
+                conv = conv + prm[j : j + 1, :] * gp[first : first + R, :]
+            snd[b] = conv.astype(BF16)
+            sts[b, 0] = to_row(jnp.sum(conv, axis=1, keepdims=True))
+            sts[b, 1] = to_row(jnp.sum(conv * conv, axis=1, keepdims=True))
+            own = (b == z) & (mine == 1)
+
+            @pl.when(own)
+            def _():
+                d_own(b, 1).start()
+
+            @pl.when(jnp.logical_not(own))
+            def _():
+                d_far(b, 1).start()
+
+            for q in range(4):
+                self_st = (b == z) & (q == tp)
+
+                @pl.when(self_st)
+                def _():
+                    s_own(b).start()
+
+                @pl.when(jnp.logical_not(self_st))
+                def _():
+                    s_far(b, q).start()
+
+    for h in range(2):
+        zs = 2 * c + h
+        for core in range(2):
+            buf = ar if core == 0 else cr
+            own = (zs == z) & (c == core)
+
+            @pl.when(own)
+            def _():
+                pltpu.make_async_copy(buf.at[h], buf.at[h], s_dr.at[core, h]).wait()
+                if core == 0:
+                    pltpu.make_async_copy(lmr.at[h], lmr.at[h], s_lr.at[h]).wait()
+
+            @pl.when(jnp.logical_not(own))
+            def _():
+                rc(buf.at[h], buf.at[h], s_ds.at[0], s_dr.at[core, h], (g, z, partner)).wait_recv()
+                if core == 0:
+                    rc(lmr.at[h], lmr.at[h], s_ls.at[0], s_lr.at[h], (g, z, partner)).wait_recv()
+
+    for xx in range(2):
+        for s in range(SP):
+            i = 4 * xx + s
+            own = (s == z) & (xx == x) & (c == 1)
+
+            @pl.when(own)
+            def _():
+                pltpu.make_async_copy(sr.at[i], sr.at[i], s_sr.at[i]).wait()
+
+            @pl.when(jnp.logical_not(own))
+            def _():
+                rc(sr.at[i], sr.at[i], s_ss.at[0, 0], s_sr.at[i], (g, z, partner)).wait_recv()
+
+    log_out[0:1, :] = lmr[0, 0:1, :]
+    log_out[1:2, :] = lmr[1, 0:1, :]
+    tot = sr[0]
+    for i in range(1, 2 * SP):
+        tot = tot + sr[i]
+    mean = to_col(tot[0, 0:1, :]) / CW
+    spread = to_col(tot[1, 0:1, :]) / CW - mean * mean
+    inv = lax.rsqrt(spread + norm_eps)
+    att = ar[0] + ar[1]
+    chans = []
+    for h in range(2):
+        v = (cr[h].astype(F32) - mean) * inv * channel_gain[:, 128 * h : 128 * h + 128] + channel_bias[
+            :, 128 * h : 128 * h + 128
+        ]
+        chans.append((v * jax.nn.sigmoid(v)).astype(BF16))
+    feats = jnp.concatenate([att] + chans, axis=1)
+    wo_a.wait()
+    wo_c.wait()
+    H = R // 2
+    n_col = 4
+    cw = D // n_col
+    for k in range(n_col):
+        cs = slice(k * cw, (k + 1) * cw)
+        mp[:, cs] = jnp.dot(feats[:, 0:128], woa[:, cs], preferred_element_type=F32) + jnp.dot(
+            feats[:, 128:384], woc[:, cs], preferred_element_type=F32
+        )
+    away = pl.ds(pl.multiple_of((1 - c) * H, H), H)
+    here = pl.ds(pl.multiple_of(c * H, H), H)
+    m_send = rc(mp.at[away, :], ma, s_ms.at[0], s_mr.at[0], (g, z, partner))
+    m_send.start()
+    m_send.wait_recv()
+    bx[...] = (mp[here, :] + ma[...]).astype(BF16)
+    b_send = rc(bx, bxr, s_bs.at[0], s_br.at[0], (g, z, across))
+    b_send.start()
+    b_send.wait_recv()
+    tot2 = bx[...].astype(F32) + bxr[...].astype(F32)
+    ms = jnp.mean(tot2 * tot2, axis=-1, keepdims=True)
+    out[here, :] = (tot2 * lax.rsqrt(ms + norm_eps) * out_gain[...]).astype(BF16)
+    e_send = rc(out.at[here, :], out.at[here, :], s_es.at[0], s_er.at[0], (g, z, partner))
+    e_send.start()
+
+    @pl.when(z < SP - 1)
+    def _():
+        x_right(z).wait_send()
+
+    @pl.when(z > 0)
+    def _():
+        x_left(z).wait_send()
+
+    for d in range(1, SP):
+
+        @pl.when(z - d >= 0)
+        def _():
+            b = z - d
+
+            @pl.when(z < SP - 1)
+            def _():
+                x_right(b).wait_send()
+
+        @pl.when(z + d < SP)
+        def _():
+            b = z + d
+
+            @pl.when(z > 0)
+            def _():
+                x_left(b).wait_send()
+
+        for sgn in (-1, 1):
+
+            @pl.when((z + sgn * d >= 0) & (z + sgn * d < SP))
+            def _():
+                b = z + sgn * d
+                x_cross(b).wait_send()
+                x_d2d(b, 0, tp).wait_send()
+                x_d2d(b, 1, across).wait_send()
+                rc(
+                    w_half(b, g), w_half(b, g), s_wys.at[b], s_wyr.at[b], (1 - g, z, tp)
+                ).wait_send()
+
+    for h in range(2):
+        for r in range(2):
+            zt = 2 * c + h
+
+            @pl.when(zt != z)
+            def _():
+                w_far(h, r).wait_send()
+
+            @pl.when((zt == z) & (c != r))
+            def _():
+                w_near(h, r).wait_send()
+
+        own = (2 * c + h == z) & (c == 0)
+
+        @pl.when(jnp.logical_not(own))
+        def _():
+            off_far(h).wait_send()
+
+    @pl.when(c == mine)
+    def _():
+        p_send.wait_send()
+
+    for t in range(SP):
+        for core in range(2):
+
+            @pl.when((c == core) & jnp.logical_not((t == z) & (mine == core)))
+            def _():
+                d_far(t, core).wait_send()
+                if core == 0:
+                    l_far(t).wait_send()
+
+        for q in range(4):
+
+            @pl.when((c == 1) & jnp.logical_not((t == z) & (q == tp)))
+            def _():
+                s_far(t, q).wait_send()
+
+    m_send.wait_send()
+    b_send.wait_send()
+    e_send.wait()
+
+
+def split_local(
+    tokens,
+    norm_gain,
+    w_query,
+    w_key,
+    w_value,
+    w_gv,
+    w_gg,
+    key_offset,
+    head_gain,
+    conv_taps,
+    channel_gain,
+    channel_bias,
+    w_oa,
+    w_oc,
+    out_gain,
+):
+    SP = lax.axis_size("sp")
+    R, D = tokens.shape
+    KS = w_query.shape[0]
+    DMA = pltpu.SemaphoreType.DMA
+    vm = pl.BlockSpec(memory_space=pltpu.VMEM)
+    hb = pl.BlockSpec(memory_space=pl.ANY)
+    V = pltpu.VMEM
+    return pl.pallas_call(
+        functools.partial(split_kernel, SP),
+        out_shape=(
+            jax.ShapeDtypeStruct((R, D), BF16),
+            jax.ShapeDtypeStruct((2, R), F32),
+        ),
+        in_specs=[vm] * 12 + [hb, hb, vm],
+        out_specs=(vm, vm),
+        scratch_shapes=[
+            V((SP * R, D), BF16),
+            V((SP * KS, 256), BF16),
+            V((2, 2, KS, 256), BF16),
+            V((40, 128), F32),
+            V((2, 8, R), F32),
+            V((SP, 8, R), F32),
+            V((SP * R, 256), BF16),
+            V((SP * R + 32, 128), F32),
+            V((SP, R, 128), BF16),
+            V((SP, 8, R), F32),
+            V((SP, 2, 8, R), F32),
+            V((2, R, 128), BF16),
+            V((2, R, 128), BF16),
+            V((2, 8, R), F32),
+            V((2 * SP, 2, 8, R), F32),
+            V(w_oa.shape, BF16),
+            V(w_oc.shape, BF16),
+            V((R, D), F32),
+            V((R // 2, D), F32),
+            V((R // 2, D), BF16),
+            V((R // 2, D), BF16),
+            DMA((2,)),
+            DMA((2, 2)),
+            DMA((SP,)),
+            DMA((SP,)),
+            DMA((SP,)),
+            DMA((SP,)),
+            DMA((SP,)),
+            DMA((SP,)),
+            DMA((SP,)),
+            DMA((SP,)),
+            DMA((SP, 2)),
+            DMA((SP, 2)),
+            DMA((1,)),
+            DMA((1,)),
+            DMA((2,)),
+            DMA((SP,)),
+            DMA((SP,)),
+            DMA((2, 2)),
+            DMA((SP,)),
+            DMA((2,)),
+            DMA((SP, 4)),
+            DMA((2 * SP,)),
+            DMA((1,)),
+            DMA((1,)),
+            DMA((1,)),
+            DMA((1,)),
+            DMA((1,)),
+            DMA((1,)),
+        ],
+        compiler_params=pltpu.CompilerParams(collective_id=0, has_side_effects=True),
+    )(
+        tokens,
+        norm_gain.reshape(1, -1),
+        w_query,
+        w_key,
+        w_value,
+        w_gv,
+        w_gg,
+        key_offset,
+        head_gain,
+        conv_taps,
+        channel_gain.reshape(1, -1),
+        channel_bias.reshape(1, -1),
+        w_oa,
+        w_oc,
+        out_gain.reshape(1, -1),
+    )
+
+
+def either(*args):
+    tokens, w_query, head_gain, conv_taps = args[0], args[2], args[8], args[9]
+    fits = (
+        lax.axis_size("grp") == 2
+        and lax.axis_size("sp") == 4
+        and lax.axis_size("tp") == 4
+        and tokens.shape[0] == 128
+        and w_query.shape[0] * 4 == tokens.shape[1]
+        and head_gain.shape == (2, 64)
+        and conv_taps.shape[1] == 256
+        and conv_taps.shape[0] <= 32
+        and args[3].shape[1] == 128
+    )
+    return split_local(*args) if fits else local(*args)
+
+
 def solution(mesh):
     in_specs = (
         P(("grp", "sp"), None),
@@ -164,4 +853,4 @@
         P(),
     )
     out_specs = (P(("grp", "sp"), None), P("tp", ("grp", "sp")))
-    return jax.shard_map(local, mesh=mesh, in_specs=in_specs, out_specs=out_specs, check_vma=False)
+    return jax.shard_map(either, mesh=mesh, in_specs=in_specs, out_specs=out_specs, check_vma=False)

time: 169 us -> 59.9 us (0.35)
  blocking collectives: 106 us -> 0 us
  Pallas kernels: 0 us -> 55.3 us
  waiting for transfers between devices: 26.9 us -> 0 us
  between operations: 14 us -> 0.66 us
  matrix products: 6.76 us -> 0 us
  other arithmetic: 5.54 us -> 0 us
  local copies, waits for them, and re-layouts: 6.76 us -> 3.83 us
  starting transfers between devices: 1.83 us -> 0 us
    all_gather x7 -> x0, blocking collectives: 101 us -> none  [the longest x1 21.4 us: local(): lax.all_gather(weights_in[1], 'sp', axis=0, tiled=True)]
    pallas_call x0 -> x1, Pallas kernels: none -> 55.3 us  [split_local(): pl.pallas_call(functools.partial(split_kernel, SP), out_shape=(jax.ShapeD...]
    reduce_scatter x1 -> x0, waiting for transfers between devices: 24.2 us -> none  [local(): lax.psum_scatter(jnp.dot(attended, w_out_attn, preferred_element_type=jnp...]
    dot_general x9 -> x0, matrix products: 6.76 us -> none  [the longest x5 4.29 us: local(): jnp.dot(normed, shard_piece, preferred_element_type=jnp.float32)]
    psum x1 -> x0, blocking collectives: 5.66 us -> none  [local(): lax.psum((jnp.sum(conv_out, axis=1), jnp.sum(conv_out * conv_out, axis=1)...]
    reduce_sum x5 -> x0, other arithmetic: 2.74 us -> none  [the longest x3 1.36 us: row_norm(): squares = jnp.mean(values_in * values_in, axis=-1, keepdims=True)]
    another operation x2 -> x0, other arithmetic: 2.4 us -> none
    unnamed x30 -> x7, local copies, waits for them, and re-layouts: 5.79 us -> 3.83 us
  transfers between devices with their start and end apart: 4 -> 0, of which waited for: 2 -> 0; matrix products, arithmetic and copies ran while one was open for 5% -> 0% of each run, Pallas kernels for 0% -> 0%
where the time goes in v1:
time: 59.9 us; the launch traced here: 59.8 us
  Pallas kernels  55.3 us (92%)
  local copies, waits for them, and re-layouts  3.83 us (6%)
  between operations  0.66 us (1%)
    pallas_call x1, Pallas kernels, split_local(): pl.pallas_call(functools.partial(split_kernel, SP), out_shape=(jax.ShapeD...  55.3 us
    unnamed x7, local copies, waits for them, and re-layouts  3.83 us

profile of v1, /device:TPU:0, one launch (start us, length us, event | category | flops | bytes accessed | tf_op | source)
XLA Modules:
  0.0 59.8 jit_solution(13756786625767560913)
XLA Ops:
  0.6 0.0 copy-start.1
  0.6 0.6 %copy-done.1 = bf16[128,2]{0,1:T(2,128)(2,1)S(1)} copy-done((bf16[128,2]{0,1:T(2,128)(2,1)S(1)}, bf16[128,2]{0,1:T(2,128)(2,1)}, u32[]{:S(2)}) %copy-start.1) | copy-done | bytes 536
  1.3 0.7 %copy.17.key_offset = bf16[128,2]{1,0:T(8,128)(2,1)} copy(bf16[128,2]{0,1:T(2,128)(2,1)S(1)} %copy-done.1) | data formatting | bytes 1024 | tf_op args[7]
  2.0 55.3 %shard_map.158 = (bf16[128,2048]{1,0:T(8,128)(2,1)}, f32[2,128]{1,0:T(2,128)}) custom-call(bf16[128,2048]{1,0:T(8,128)(2,1)} %tokens.1, f32[1,2048]{1,0:T(1,128)} %bitcast.4, bf16[512,128]{1,0:T(8,128)(2,1)} %w_query.1, bf16[512,128]{1,0:T(8,128)(2,1)} %w_key.1, bf16[512,128]{1,0:T(8,128)(2,1)} %w_value.1, bf16[512,256]{1,0:T(8,128)(2,1)} %w_gv.1, ...), custom_call_target="tpu_custom_call" | custom-call | tf_op jit(solution)/shard_map/pallas_call | solution.py:742
  57.3 0.0 copy-start
  57.3 1.9 %copy.20 = bf16[128,2048]{1,0:T(8,128)(2,1)} copy(bf16[128,2048]{1,0:T(8,128)(2,1)} %get-tuple-element.4) | data formatting | bytes 1048576
  59.2 0.0 copy-done
  59.2 0.6 copy.21
Async XLA Ops:
  0.6 0.7 %copy-start.1 = (bf16[128,2]{0,1:T(2,128)(2,1)S(1)}, bf16[128,2]{0,1:T(2,128)(2,1)}, u32[]{:S(2)}) copy-start(bf16[128,2]{0,1:T(2,128)(2,1)} %param.22) | copy-start | bytes 1540
  57.3 1.9 %copy-start = (f32[2,128]{1,0:T(2,128)S(1)}, f32[2,128]{1,0:T(2,128)}, u32[]{:S(2)}) copy-start(f32[2,128]{1,0:T(2,128)} %get-tuple-element.5) | copy-start | bytes 3076

commit v2 on v1

--- a/solution.py
+++ b/solution.py
@@ -222,6 +222,10 @@
     s_br,
     s_es,
     s_er,
+    tokv,
+    wqv,
+    wkv,
+    s_in,
 ):
     g = lax.axis_index("grp")
     z = lax.axis_index("sp")
@@ -233,6 +237,7 @@
     diag = 2 * (1 - x) + (1 - c)
     mine = z // 2
     par = z % 2
+    NS = 2
     R = tokens.shape[0]
     D = tokens.shape[1]
     KS = w_query.shape[0]
@@ -245,10 +250,22 @@
             src_ref=src, dst_ref=dst, send_sem=ss, recv_sem=rs, device_id=dev, device_id_type=MESH
         )
 
+    def cp(src, dst, i):
+        return pltpu.make_async_copy(src, dst, s_in.at[i])
+
+    in_tok = cp(tokens, tokv, 0)
+    in_q = cp(w_query, wqv, 1)
+    in_k = cp(w_key, wkv, 2)
+    in_w = []
+    for h in range(2):
+        lanes = slice(128 * h, 128 * h + 128)
+        in_w.append(cp(w_value, stg.at[h, 0, :, 128:256], 3 + 3 * h))
+        in_w.append(cp(w_gv.at[:, lanes], stg.at[h, 1, :, 0:128], 4 + 3 * h))
+        in_w.append(cp(w_gg.at[:, lanes], stg.at[h, 1, :, 128:256], 5 + 3 * h))
     wo_a = pltpu.make_async_copy(w_oa, woa, s_wo.at[0])
     wo_c = pltpu.make_async_copy(w_oc, woc, s_wo.at[1])
-    wo_a.start()
-    wo_c.start()
+    for copy in [in_tok, in_q, in_k] + in_w + [wo_a, wo_c]:
+        copy.start()
 
     barrier = pltpu.get_barrier_semaphore()
     for dz in range(SP):
@@ -260,46 +277,57 @@
             )
     pl.semaphore_signal(barrier, inc=1, device_id=(1 - g, z, tp), device_id_type=MESH)
 
-    t32 = tokens[...].astype(F32)
+    in_tok.wait()
+    t32 = tokv[...].astype(F32)
     sq = jnp.mean(t32 * t32, axis=-1, keepdims=True)
     X[pl.ds(pl.multiple_of(z * R, R), R), :] = (
         t32 * lax.rsqrt(sq + norm_eps) * norm_gain[...]
     ).astype(BF16)
     pl.semaphore_wait(barrier, SP * 4)
 
-    def xs(block, quarter):
-        return X.at[pl.ds(pl.multiple_of(block * R + quarter * Q, Q), Q), :]
-
-    def x_right(b):
-        return rc(xs(b, tp), xs(b, tp), s_xrt.at[b], s_xr.at[b], (g, jnp.minimum(z + 1, SP - 1), tp))
-
-    def x_left(b):
-        return rc(xs(b, tp), xs(b, tp), s_xl.at[b], s_xr.at[b], (g, jnp.maximum(z - 1, 0), tp))
-
-    def x_cross(b):
-        return rc(xs(b, tp), xs(b, tp), s_xxs.at[b], s_xxr.at[b], (g, z, across))
-
-    def x_cross_in(b):
-        return rc(xs(b, across), xs(b, across), s_xxs.at[b], s_xxr.at[b], (g, z, across))
-
-    def x_d2d(b, k, quarter):
-        return rc(xs(b, quarter), xs(b, quarter), s_xds.at[b, k], s_xdr.at[b, k], (g, z, partner))
-
-    @pl.when(z < SP - 1)
-    def _():
-        x_right(z).start()
-
-    @pl.when(z > 0)
-    def _():
-        x_left(z).start()
-
+    QS = Q // NS
+
+    def xs(block, quarter, u):
+        return X.at[pl.ds(pl.multiple_of(block * R + quarter * Q + u * QS, QS), QS), :]
+
+    def x_right(b, u):
+        r = xs(b, tp, u)
+        return rc(r, r, s_xrt.at[b, u], s_xr.at[b, u], (g, jnp.minimum(z + 1, SP - 1), tp))
+
+    def x_left(b, u):
+        r = xs(b, tp, u)
+        return rc(r, r, s_xl.at[b, u], s_xr.at[b, u], (g, jnp.maximum(z - 1, 0), tp))
+
+    def x_cross(b, u):
+        r = xs(b, tp, u)
+        return rc(r, r, s_xxs.at[b, u], s_xxr.at[b, u], (g, z, across))
+
+    def x_cross_in(b, u):
+        r = xs(b, across, u)
+        return rc(r, r, s_xxs.at[b, u], s_xxr.at[b, u], (g, z, across))
+
+    def x_d2d(b, k, quarter, u):
+        r = xs(b, quarter, u)
+        return rc(r, r, s_xds.at[b, k, u], s_xdr.at[b, k, u], (g, z, partner))
+
+    for u in range(NS):
+
+        @pl.when(z < SP - 1)
+        def _():
+            x_right(z, u).start()
+
+        @pl.when(z > 0)
+        def _():
+            x_left(z, u).start()
+
+    in_q.wait()
+    in_k.wait()
     for h in range(2):
         stg[h, 0, :, 0:128] = jnp.concatenate(
-            [w_query[:, 64 * h : 64 * h + 64], w_key[:, 64 * h : 64 * h + 64]], axis=1
+            [wqv[:, 64 * h : 64 * h + 64], wkv[:, 64 * h : 64 * h + 64]], axis=1
         )
-        stg[h, 0, :, 128:256] = w_value[...]
-        stg[h, 1, :, 0:128] = w_gv[:, 128 * h : 128 * h + 128]
-        stg[h, 1, :, 128:256] = w_gg[:, 128 * h : 128 * h + 128]
+    for copy in in_w:
+        copy.wait()
 
     def w_half(b, part):
         return WA.at[pl.ds(pl.multiple_of(b * KS + part * KH, KH), KH), :]
@@ -322,7 +350,7 @@
     def w_own(h, r):
         return pltpu.make_async_copy(stg.at[h, r], w_full(z), s_wr.at[z])
 
-    for h in range(2):
+    def send_w(h):
         for r in range(2):
             zt = 2 * c + h
 
@@ -337,6 +365,9 @@
             @pl.when((zt == z) & (c == r))
             def _():
                 w_own(h, r).start()
+
+    send_w(0)
+    send_w(1)
 
     eye = lax.broadcasted_iota(jnp.int32, (R, R), 0) == lax.broadcasted_iota(jnp.int32, (R, R), 1)
 
@@ -356,7 +387,7 @@
 
     ko = key_offset[...].astype(F32)
     for h in range(2):
-        offs[h] = to_row(ko[:, h : h + 1])
+        offs[h] = jnp.broadcast_to(ko[h : h + 1, :], (8, R))
         own = (2 * c + h == z) & (c == 0)
 
         @pl.when(own)
@@ -376,48 +407,65 @@
         prm[32:33, :] = jnp.concatenate([head_gain[0:1, :], head_gain[1:2, :]], axis=1)
         p_send.start()
 
-    for d in range(1, SP):
-
-        @pl.when(z - d >= 0)
-        def _():
-            b = z - d
-            x_left(b).wait_recv()
-
-            @pl.when(z < SP - 1)
-            def _():
-                x_right(b).start()
-
-            x_cross(b).start()
-            x_d2d(b, 0, tp).start()
-
-        @pl.when(z + d < SP)
-        def _():
-            b = z + d
-            x_left(b).wait_recv()
-
-            @pl.when(z > 0)
-            def _():
-                x_left(b).start()
-
-            x_cross(b).start()
-            x_d2d(b, 0, tp).start()
-
+    def take_z(d):
+        for u in range(NS):
+
+            @pl.when(z - d >= 0)
+            def _():
+                b = z - d
+                x_left(b, u).wait_recv()
+
+                @pl.when(z < SP - 1)
+                def _():
+                    x_right(b, u).start()
+
+                x_cross(b, u).start()
+                x_d2d(b, 0, tp, u).start()
+
+            @pl.when(z + d < SP)
+            def _():
+                b = z + d
+                x_left(b, u).wait_recv()
+
+                @pl.when(z > 0)
+                def _():
+                    x_left(b, u).start()
+
+                x_cross(b, u).start()
+                x_d2d(b, 0, tp, u).start()
+
+    def both(d, body):
         for sgn in (-1, 1):
 
             @pl.when((z + sgn * d >= 0) & (z + sgn * d < SP))
             def _():
-                b = z + sgn * d
-                x_cross_in(b).wait_recv()
-                x_d2d(b, 1, across).start()
-
-        for sgn in (-1, 1):
-
-            @pl.when((z + sgn * d >= 0) & (z + sgn * d < SP))
-            def _():
-                b = z + sgn * d
-                w = rc(w_half(b, g), w_half(b, g), s_wys.at[b], s_wr.at[b], (1 - g, z, tp))
-                w.wait_recv()
-                rc(w_half(b, g), w_half(b, g), s_wys.at[b], s_wyr.at[b], (1 - g, z, tp)).start()
+                body(z + sgn * d)
+
+    def take_x(d):
+        def body(b):
+            for u in range(NS):
+                x_cross_in(b, u).wait_recv()
+                x_d2d(b, 1, across, u).start()
+
+        both(d, body)
+
+    def take_w(d):
+        def body(b):
+            w = rc(w_half(b, g), w_half(b, g), s_wys.at[b], s_wr.at[b], (1 - g, z, tp))
+            w.wait_recv()
+            rc(w_half(b, g), w_half(b, g), s_wys.at[b], s_wyr.at[b], (1 - g, z, tp)).start()
+
+        both(d, body)
+
+    take_z(1)
+    take_w(1)
+    take_x(1)
+    take_z(2)
+    take_w(2)
+    take_x(2)
+    take_z(3)
+    take_w(3)
+    take_x(3)
 
     @pl.when(c == mine)
     def _():
@@ -434,8 +482,9 @@
             @pl.when((z + sgn * d >= 0) & (z + sgn * d < SP))
             def _():
                 b = z + sgn * d
-                x_d2d(b, 0, partner).wait_recv()
-                x_d2d(b, 1, diag).wait_recv()
+                for u in range(NS):
+                    x_d2d(b, 0, partner, u).wait_recv()
+                    x_d2d(b, 1, diag, u).wait_recv()
                 rc(
                     w_half(b, 1 - g), w_half(b, 1 - g), s_wys.at[b], s_wyr.at[b], (1 - g, z, tp)
                 ).wait_recv()
@@ -615,63 +664,65 @@
     H = R // 2
     n_col = 4
     cw = D // n_col
+    away = pl.ds(pl.multiple_of((1 - c) * H, H), H)
+    here = pl.ds(pl.multiple_of(c * H, H), H)
+
+    def m_send(k):
+        cs = slice(k * cw, (k + 1) * cw)
+        return rc(mp.at[away, cs], ma.at[:, cs], s_ms.at[k], s_mr.at[k], (g, z, partner))
+
+    def b_send(k):
+        cs = slice(k * cw, (k + 1) * cw)
+        return rc(bx.at[:, cs], bxr.at[:, cs], s_bs.at[k], s_br.at[k], (g, z, across))
+
     for k in range(n_col):
         cs = slice(k * cw, (k + 1) * cw)
         mp[:, cs] = jnp.dot(feats[:, 0:128], woa[:, cs], preferred_element_type=F32) + jnp.dot(
             feats[:, 128:384], woc[:, cs], preferred_element_type=F32
         )
-    away = pl.ds(pl.multiple_of((1 - c) * H, H), H)
-    here = pl.ds(pl.multiple_of(c * H, H), H)
-    m_send = rc(mp.at[away, :], ma, s_ms.at[0], s_mr.at[0], (g, z, partner))
-    m_send.start()
-    m_send.wait_recv()
-    bx[...] = (mp[here, :] + ma[...]).astype(BF16)
-    b_send = rc(bx, bxr, s_bs.at[0], s_br.at[0], (g, z, across))
-    b_send.start()
-    b_send.wait_recv()
+        m_send(k).start()
+    for k in range(n_col):
+        cs = slice(k * cw, (k + 1) * cw)
+        m_send(k).wait_recv()
+        bx[:, cs] = (mp[here, cs] + ma[:, cs]).astype(BF16)
+        b_send(k).start()
+    for k in range(n_col):
+        b_send(k).wait_recv()
     tot2 = bx[...].astype(F32) + bxr[...].astype(F32)
     ms = jnp.mean(tot2 * tot2, axis=-1, keepdims=True)
     out[here, :] = (tot2 * lax.rsqrt(ms + norm_eps) * out_gain[...]).astype(BF16)
     e_send = rc(out.at[here, :], out.at[here, :], s_es.at[0], s_er.at[0], (g, z, partner))
     e_send.start()
 
-    @pl.when(z < SP - 1)
-    def _():
-        x_right(z).wait_send()
-
-    @pl.when(z > 0)
-    def _():
-        x_left(z).wait_send()
+    for u in range(NS):
+
+        @pl.when(z < SP - 1)
+        def _():
+            x_right(z, u).wait_send()
+
+        @pl.when(z > 0)
+        def _():
+            x_left(z, u).wait_send()
 
     for d in range(1, SP):
-
-        @pl.when(z - d >= 0)
-        def _():
-            b = z - d
-
-            @pl.when(z < SP - 1)
-            def _():
-                x_right(b).wait_send()
-
-        @pl.when(z + d < SP)
-        def _():
-            b = z + d
-
-            @pl.when(z > 0)
-            def _():
-                x_left(b).wait_send()
-
-        for sgn in (-1, 1):
-
-            @pl.when((z + sgn * d >= 0) & (z + sgn * d < SP))
-            def _():
-                b = z + sgn * d
-                x_cross(b).wait_send()
-                x_d2d(b, 0, tp).wait_send()
-                x_d2d(b, 1, across).wait_send()
-                rc(
-                    w_half(b, g), w_half(b, g), s_wys.at[b], s_wyr.at[b], (1 - g, z, tp)
-                ).wait_send()
+        for u in range(NS):
+
+            @pl.when((z - d >= 0) & (z < SP - 1))
+            def _():
+                x_right(z - d, u).wait_send()
+
+            @pl.when((z + d < SP) & (z > 0))
+            def _():
+                x_left(z + d, u).wait_send()
+
+        def drain(b):
+            for u in range(NS):
+                x_cross(b, u).wait_send()
+                x_d2d(b, 0, tp, u).wait_send()
+                x_d2d(b, 1, across, u).wait_send()
+            rc(w_half(b, g), w_half(b, g), s_wys.at[b], s_wyr.at[b], (1 - g, z, tp)).wait_send()
+
+        both(d, drain)
 
     for h in range(2):
         for r in range(2):
@@ -710,8 +761,9 @@
             def _():
                 s_far(t, q).wait_send()
 
-    m_send.wait_send()
-    b_send.wait_send()
+    for k in range(n_col):
+        m_send(k).wait_send()
+        b_send(k).wait_send()
     e_send.wait()
 
 
@@ -745,7 +797,7 @@
             jax.ShapeDtypeStruct((R, D), BF16),
             jax.ShapeDtypeStruct((2, R), F32),
         ),
-        in_specs=[vm] * 12 + [hb, hb, vm],
+        in_specs=[hb, vm] + [hb] * 5 + [vm] * 5 + [hb, hb, vm],
         out_specs=(vm, vm),
         scratch_shapes=[
             V((SP * R, D), BF16),
@@ -774,13 +826,13 @@
             DMA((SP,)),
             DMA((SP,)),
             DMA((SP,)),
-            DMA((SP,)),
-            DMA((SP,)),
-            DMA((SP,)),
-            DMA((SP,)),
-            DMA((SP,)),
             DMA((SP, 2)),
             DMA((SP, 2)),
+            DMA((SP, 2)),
+            DMA((SP, 2)),
+            DMA((SP, 2)),
+            DMA((SP, 2, 2)),
+            DMA((SP, 2, 2)),
             DMA((1,)),
             DMA((1,)),
             DMA((2,)),
@@ -791,12 +843,16 @@
             DMA((2,)),
             DMA((SP, 4)),
             DMA((2 * SP,)),
+            DMA((4,)),
+            DMA((4,)),
+            DMA((4,)),
+            DMA((4,)),
             DMA((1,)),
             DMA((1,)),
-            DMA((1,)),
-            DMA((1,)),
-            DMA((1,)),
-            DMA((1,)),
+            V((R, D), BF16),
+            V(w_query.shape, BF16),
+            V(w_key.shape, BF16),
+            DMA((9,)),
         ],
         compiler_params=pltpu.CompilerParams(collective_id=0, has_side_effects=True),
     )(
@@ -807,7 +863,7 @@
         w_value,
         w_gv,
         w_gg,
-        key_offset,
+        key_offset.T,
         head_gain,
         conv_taps,
         channel_gain.reshape(1, -1),

time: 59.9 us -> 54.5 us (0.910)
  Pallas kernels: 55.3 us -> 51.2 us
  local copies, waits for them, and re-layouts: 3.83 us -> 2.45 us
    pallas_call x1, Pallas kernels: 55.3 us -> 51.2 us  [split_local(): pl.pallas_call(functools.partial(split_kernel, SP), out_shape=(jax.ShapeD...]
    unnamed x7 -> x4, local copies, waits for them, and re-layouts: 3.83 us -> 2.45 us
where the time goes in v2:
time: 54.5 us; the launch traced here: 54.3 us
  Pallas kernels  51.2 us (94%)
  local copies, waits for them, and re-layouts  2.45 us (4%)
  between operations  0.65 us (1%)
    pallas_call x1, Pallas kernels, split_local(): pl.pallas_call(functools.partial(split_kernel, SP), out_shape=(jax.ShapeD...  51.2 us
    unnamed x4, local copies, waits for them, and re-layouts  2.45 us

profile of v2, /device:TPU:0, one launch (start us, length us, event | category | flops | bytes accessed | tf_op | source)
XLA Modules:
  0.0 54.3 jit_solution(14758501954806251760)
XLA Ops:
  0.6 51.2 %shard_map.158 = (bf16[128,2048]{1,0:T(8,128)(2,1)}, f32[2,128]{1,0:T(2,128)}) custom-call(bf16[128,2048]{1,0:T(8,128)(2,1)} %tokens.1, f32[1,2048]{1,0:T(1,128)} %bitcast.5, bf16[512,128]{1,0:T(8,128)(2,1)} %w_query.1, bf16[512,128]{1,0:T(8,128)(2,1)} %w_key.1, bf16[512,128]{1,0:T(8,128)(2,1)} %w_value.1, bf16[512,256]{1,0:T(8,128)(2,1)} %w_gv.1, ...), custom_call_target="tpu_custom_call" | custom-call | tf_op jit(solution)/shard_map/pallas_call | solution.py:794
  51.9 0.0 copy-start
  51.9 1.9 %copy.19 = bf16[128,2048]{1,0:T(8,128)(2,1)} copy(bf16[128,2048]{1,0:T(8,128)(2,1)} %get-tuple-element.4) | data formatting | bytes 1048576
  53.8 0.0 copy-done
  53.8 0.6 %copy.20 = f32[2,128]{1,0:T(2,128)} copy(f32[2,128]{1,0:T(2,128)S(1)} %copy-done) | data formatting | bytes 2048
Async XLA Ops:
  51.9 1.9 %copy-start = (f32[2,128]{1,0:T(2,128)S(1)}, f32[2,128]{1,0:T(2,128)}, u32[]{:S(2)}) copy-start(f32[2,128]{1,0:T(2,128)} %get-tuple-element.5) | copy-start | bytes 3076

commit v3 on v2

--- a/solution.py
+++ b/solution.py
@@ -329,26 +329,28 @@
     for copy in in_w:
         copy.wait()
 
-    def w_half(b, part):
-        return WA.at[pl.ds(pl.multiple_of(b * KS + part * KH, KH), KH), :]
+    KW = KH // NS
+
+    def w_half(b, part, u):
+        return WA.at[pl.ds(pl.multiple_of(b * KS + part * KH + u * KW, KW), KW), :]
 
     def w_full(b):
         return WA.at[pl.ds(pl.multiple_of(b * KS, KS), KS), :]
 
-    def w_far(h, r):
+    def w_far(h, r, u):
         return rc(
-            stg.at[h, r, pl.ds(pl.multiple_of(g * KH, KH), KH), :],
-            w_half(z, g),
-            s_ws.at[h, r],
-            s_wr.at[z],
+            stg.at[h, r, pl.ds(pl.multiple_of(g * KH + u * KW, KW), KW), :],
+            w_half(z, g, u),
+            s_ws.at[h, r, u],
+            s_wr.at[z, u],
             (g, 2 * c + h, 2 * x + r),
         )
 
     def w_near(h, r):
-        return rc(stg.at[h, r], w_full(z), s_ws.at[h, r], s_wr.at[z], (g, z, partner))
+        return rc(stg.at[h, r], w_full(z), s_ws.at[h, r, 0], s_wr.at[z, 0], (g, z, partner))
 
     def w_own(h, r):
-        return pltpu.make_async_copy(stg.at[h, r], w_full(z), s_wr.at[z])
+        return pltpu.make_async_copy(stg.at[h, r], w_full(z), s_wr.at[z, 0])
 
     def send_w(h):
         for r in range(2):
@@ -356,7 +358,8 @@
 
             @pl.when(zt != z)
             def _():
-                w_far(h, r).start()
+                for u in range(NS):
+                    w_far(h, r, u).start()
 
             @pl.when((zt == z) & (c != r))
             def _():
@@ -366,8 +369,15 @@
             def _():
                 w_own(h, r).start()
 
-    send_w(0)
-    send_w(1)
+    @pl.when(2 * z >= SP)
+    def _():
+        send_w(0)
+        send_w(1)
+
+    @pl.when(2 * z < SP)
+    def _():
+        send_w(1)
+        send_w(0)
 
     eye = lax.broadcasted_iota(jnp.int32, (R, R), 0) == lax.broadcasted_iota(jnp.int32, (R, R), 1)
 
@@ -451,29 +461,30 @@
 
     def take_w(d):
         def body(b):
-            w = rc(w_half(b, g), w_half(b, g), s_wys.at[b], s_wr.at[b], (1 - g, z, tp))
-            w.wait_recv()
-            rc(w_half(b, g), w_half(b, g), s_wys.at[b], s_wyr.at[b], (1 - g, z, tp)).start()
+            for u in range(NS):
+                w = w_half(b, g, u)
+                rc(w, w, s_wys.at[b, u], s_wr.at[b, u], (1 - g, z, tp)).wait_recv()
+                rc(w, w, s_wys.at[b, u], s_wyr.at[b, u], (1 - g, z, tp)).start()
 
         both(d, body)
 
     take_z(1)
     take_w(1)
+    take_z(2)
     take_x(1)
-    take_z(2)
     take_w(2)
+    take_z(3)
     take_x(2)
-    take_z(3)
     take_w(3)
     take_x(3)
 
     @pl.when(c == mine)
     def _():
-        pltpu.make_async_copy(w_full(z), w_full(z), s_wr.at[z]).wait()
+        pltpu.make_async_copy(w_full(z), w_full(z), s_wr.at[z, 0]).wait()
 
     @pl.when(c != mine)
     def _():
-        rc(w_full(z), w_full(z), s_ws.at[0, 0], s_wr.at[z], (g, z, partner)).wait_recv()
+        rc(w_full(z), w_full(z), s_ws.at[0, 0, 0], s_wr.at[z, 0], (g, z, partner)).wait_recv()
         p_send.wait_recv()
 
     for d in range(1, SP):
@@ -485,9 +496,9 @@
                 for u in range(NS):
                     x_d2d(b, 0, partner, u).wait_recv()
                     x_d2d(b, 1, diag, u).wait_recv()
-                rc(
-                    w_half(b, 1 - g), w_half(b, 1 - g), s_wys.at[b], s_wyr.at[b], (1 - g, z, tp)
-                ).wait_recv()
+                for u in range(NS):
+                    w = w_half(b, 1 - g, u)
+                    rc(w, w, s_wys.at[b, u], s_wyr.at[b, u], (1 - g, z, tp)).wait_recv()
 
     for b in range(SP):
         proj[b * R : b * R + R, :] = jnp.dot(
@@ -720,7 +731,9 @@
                 x_cross(b, u).wait_send()
                 x_d2d(b, 0, tp, u).wait_send()
                 x_d2d(b, 1, across, u).wait_send()
-            rc(w_half(b, g), w_half(b, g), s_wys.at[b], s_wyr.at[b], (1 - g, z, tp)).wait_send()
+            for u in range(NS):
+                w = w_half(b, g, u)
+                rc(w, w, s_wys.at[b, u], s_wyr.at[b, u], (1 - g, z, tp)).wait_send()
 
         both(d, drain)
 
@@ -730,7 +743,8 @@
 
             @pl.when(zt != z)
             def _():
-                w_far(h, r).wait_send()
+                for u in range(NS):
+                    w_far(h, r, u).wait_send()
 
             @pl.when((zt == z) & (c != r))
             def _():
@@ -822,10 +836,10 @@
             V((R // 2, D), BF16),
             V((R // 2, D), BF16),
             DMA((2,)),
-            DMA((2, 2)),
-            DMA((SP,)),
-            DMA((SP,)),
-            DMA((SP,)),
+            DMA((2, 2, 2)),
+            DMA((SP, 2)),
+            DMA((SP, 2)),
+            DMA((SP, 2)),
             DMA((SP, 2)),
             DMA((SP, 2)),
             DMA((SP, 2)),

time: 54.5 us -> 55.8 us (1.024)
  Pallas kernels: 51.2 us -> 52.4 us
    pallas_call x1, Pallas kernels: 51.2 us -> 52.4 us  [split_local(): pl.pallas_call(functools.partial(split_kernel, SP), out_shape=(jax.ShapeD...]
where the time goes in v3:
time: 55.8 us; the launch traced here: 55.5 us
  Pallas kernels  52.4 us (94%)
  local copies, waits for them, and re-layouts  2.45 us (4%)
  between operations  0.65 us (1%)
    pallas_call x1, Pallas kernels, split_local(): pl.pallas_call(functools.partial(split_kernel, SP), out_shape=(jax.ShapeD...  52.4 us
    unnamed x4, local copies, waits for them, and re-layouts  2.45 us

profile of v3, /device:TPU:0, one launch (start us, length us, event | category | flops | bytes accessed | tf_op | source)
XLA Modules:
  0.0 55.5 jit_solution(11610804363842725610)
XLA Ops:
  0.6 52.4 %shard_map.158 = (bf16[128,2048]{1,0:T(8,128)(2,1)}, f32[2,128]{1,0:T(2,128)}) custom-call(bf16[128,2048]{1,0:T(8,128)(2,1)} %tokens.1, f32[1,2048]{1,0:T(1,128)} %bitcast.5, bf16[512,128]{1,0:T(8,128)(2,1)} %w_query.1, bf16[512,128]{1,0:T(8,128)(2,1)} %w_key.1, bf16[512,128]{1,0:T(8,128)(2,1)} %w_value.1, bf16[512,256]{1,0:T(8,128)(2,1)} %w_gv.1, ...), custom_call_target="tpu_custom_call" | custom-call | tf_op jit(solution)/shard_map/pallas_call | solution.py:808
  53.1 0.0 copy-start
  53.1 1.9 %copy.19 = bf16[128,2048]{1,0:T(8,128)(2,1)} copy(bf16[128,2048]{1,0:T(8,128)(2,1)} %get-tuple-element.4) | data formatting | bytes 1048576
  55.0 0.0 copy-done
  55.0 0.6 %copy.20 = f32[2,128]{1,0:T(2,128)} copy(f32[2,128]{1,0:T(2,128)S(1)} %copy-done) | data formatting | bytes 2048
Async XLA Ops:
  53.1 1.9 %copy-start = (f32[2,128]{1,0:T(2,128)S(1)}, f32[2,128]{1,0:T(2,128)}, u32[]{:S(2)}) copy-start(f32[2,128]{1,0:T(2,128)} %get-tuple-element.5) | copy-start | bytes 3076
